TPU v7x, 256 devices: a whole 4x4x8 slice. The times are simulated.
256 devices in a mesh: fs: 16 (over y, x), tp: 16 (over z, core).
Axes of the slice: x: 4, y: 4, z: 8, core: 2. Of those that a mesh axis runs over, the one named last changes fastest.
Arguments:
- normed_inputs: bfloat16 [16384, 4096], P('fs', 'tp'), may hold values from -6 to 6
- query_upstream: bfloat16 [16384, 4096], P('fs', 'tp'), may hold values from -0.0625 to 0.0625
- key_upstream: bfloat16 [16384, 1024], P('fs', 'tp'), may hold values from -0.046875 to 0.046875
- head_outputs: bfloat16 [16384, 4096], P('fs', 'tp'), may hold values from -6 to 6
- branch_upstream: bfloat16 [16384, 4096], P('fs', 'tp'), may hold values from -0.0625 to 0.0625
- query_master: float32 [4096, 4096], P('fs', 'tp'), may hold values from -0.09375 to 0.09375
- key_master: float32 [4096, 1024], P('fs', 'tp'), may hold values from -0.09375 to 0.09375
- branch_master: float32 [4096, 4096], P('fs', 'tp'), may hold values from -0.09375 to 0.09375
- query_basis: bfloat16 [4096, 128], replicated, may hold values from -0.09375 to 0.09375
- key_basis: bfloat16 [4096, 128], replicated, may hold values from -0.09375 to 0.09375
- branch_basis: bfloat16 [4096, 128], replicated, may hold values from -0.09375 to 0.09375
- query_first: float32 [128, 4096], P(None, 'tp'), may hold values from -0.75 to 0.75
- query_second: float32 [128, 4096], P(None, 'tp'), may hold values from 0.001 to 0.02
- key_first: float32 [128, 1024], P(None, 'tp'), may hold values from -0.75 to 0.75
- key_second: float32 [128, 1024], P(None, 'tp'), may hold values from 0.001 to 0.02
- branch_first: float32 [4096, 128], P('fs'), may hold values from -0.75 to 0.75
- branch_second: float32 [4096, 128], P('fs'), may hold values from 0.001 to 0.02
Outputs:
- query_step: float32 [4096, 4096], P('fs', 'tp')
- key_step: float32 [4096, 1024], P('fs', 'tp')
- branch_step: float32 [4096, 4096], P('fs', 'tp')
- query_updated: float32 [4096, 4096], P('fs', 'tp')
- key_updated: float32 [4096, 1024], P('fs', 'tp')
- branch_updated: float32 [4096, 4096], P('fs', 'tp')
- query_copy: bfloat16 [4096, 4096], P(None, 'tp')
- key_copy: bfloat16 [4096, 1024], P(None, 'tp')
- branch_copy: bfloat16 [4096, 4096], P(None, 'tp')
- query_first_new: float32 [128, 4096], P(None, 'tp')
- query_second_new: float32 [128, 4096], P(None, 'tp')
- key_first_new: float32 [128, 1024], P(None, 'tp')
- key_second_new: float32 [128, 1024], P(None, 'tp')
- branch_first_new: float32 [4096, 128], P('fs')
- branch_second_new: float32 [4096, 128], P('fs')
All inputs are finite; a program needn't handle non-finite values.
Results may differ from a plain program's by a relative error of at most 0.001.
Values may be sent and summed in bfloat16 or wider, within the bound.
A program may use at most 128 MiB of HBM per device.

v0:
```python
import functools

import jax
import jax.numpy as jnp
from jax import lax
from jax.sharding import Mesh
from jax.sharding import PartitionSpec as P

FS = ("fs_0", "fs_1")
TP = ("tp_0", "tp_1")
FS_TP = ("fs_0", "fs_1", "tp_0", "tp_1")


LEARN = 0.02
BETA_ONE = 0.9
BETA_TWO = 0.95
ADAM_EPS = 1e-08
CLIP_RMS = 0.5


def together(arrays, axis):
    vector, at, outs = (jnp.concatenate([a.reshape(-1) for a in arrays]), 0, [])
    subtotal = lax.psum(vector, axis)
    for a in arrays:
        outs.append(subtotal[at : at + a.size].reshape(a.shape))
        at += a.size
    return tuple(outs)


def in_blocks(array, dim, length):
    shape = array.shape
    pieces = array.reshape(*shape[:dim], length, shape[dim] // length, *shape[dim + 1 :])
    return jnp.moveaxis(pieces, dim, 0)


def sum_at_owner(array, axis, dim):
    pieces = in_blocks(array, dim, lax.axis_size(axis))
    arrived = lax.all_to_all(pieces, axis, split_axis=0, concat_axis=0, tiled=True)
    return arrived.sum(axis=0)


def copy_for_each(array, axis):
    length = lax.axis_size(axis)
    return lax.all_to_all(
        jnp.broadcast_to(array[None], (length, *array.shape)), axis, 0, 0, tiled=True
    )


def of_everyone(array, axis):
    return copy_for_each(array, axis).sum(axis=0)


def packed_total(arrays, axis):
    ends = [0]
    for a in arrays:
        ends.append(ends[-1] + a.size)
    subtotal = of_everyone(jnp.concatenate([a.ravel() for a in arrays]), axis)
    return tuple((subtotal[b:e].reshape(a.shape) for a, b, e in zip(arrays, ends, ends[1:])))


def gathered_total(array, axis):
    pieces = lax.all_gather(array, axis)
    return pieces.sum(axis=0)


def over_axes(array, axes):
    return functools.reduce(lax.psum, axes, array)


def in_one_piece(arrays, axis, dim, along):
    ends, at = ([], 0)
    for a in arrays[:-1]:
        at += a.shape[along]
        ends.append(at)
    both = jnp.concatenate(arrays, axis=along)
    return tuple(jnp.split(lax.all_gather(both, axis, axis=dim, tiled=True), ends, axis=along))


def moments(first, second, low, clip):
    scaled = clip * low
    first_new = BETA_ONE * first + (1.0 - BETA_ONE) * scaled
    second_new = BETA_TWO * second + (1.0 - BETA_TWO) * scaled * scaled
    return (first_new, second_new, first_new / (jnp.sqrt(second_new) + ADAM_EPS))


def over_tokens(left, right, precision=None):
    return lax.dot_general(
        left,
        right,
        (((0,), (0,)), ((), ())),
        precision=precision,
        preferred_element_type=jnp.float32,
    )


def per_device(
    normed_inputs,
    query_upstream,
    key_upstream,
    head_outputs,
    branch_upstream,
    query_master,
    key_master,
    branch_master,
    query_basis,
    key_basis,
    branch_basis,
    query_first,
    query_second,
    key_first,
    key_second,
    branch_first,
    branch_second,
):
    exact = lax.Precision.HIGHEST
    row_index = lax.axis_index(FS)
    col_index = lax.axis_index(TP)
    n_rows = lax.axis_size(FS)
    n_cols = lax.axis_size(TP)
    features = normed_inputs.shape[1]
    query_local = query_upstream.shape[1]
    key_local = key_upstream.shape[1]
    rows_in = query_master.shape[0]
    rank = query_basis.shape[1]
    whole_values = lax.all_gather(head_outputs, TP, axis=1, tiled=True)
    block_query = lax.dynamic_slice_in_dim(query_basis, col_index * features, features, 0)
    block_key = lax.dynamic_slice_in_dim(key_basis, col_index * features, features, 0)
    proj_query, proj_key = together(
        (
            jnp.dot(normed_inputs, block_query, preferred_element_type=jnp.float32),
            jnp.dot(normed_inputs, block_key, preferred_element_type=jnp.float32),
        ),
        TP,
    )
    part_query = over_tokens(proj_query, query_upstream.astype(jnp.float32), exact)
    part_key = over_tokens(proj_key, key_upstream.astype(jnp.float32), exact)
    grad_branch = sum_at_owner(over_tokens(whole_values, branch_upstream), FS, 0)
    own_branch = lax.dynamic_slice_in_dim(branch_basis, col_index * features, features, 0).astype(
        jnp.float32
    )
    part_branch = jnp.dot(grad_branch, own_branch, precision=exact)
    query_low, key_low = packed_total((part_query, part_key), FS)
    branch_low = gathered_total(part_branch, TP)
    local_squares = (jnp.sum(query_low * query_low) + jnp.sum(key_low * key_low)) / n_rows
    local_squares = local_squares + jnp.sum(branch_low * branch_low) / n_cols
    total = over_axes(local_squares, FS_TP)
    entries = rank * n_cols * (2 * query_local + key_local)
    rms_value = jnp.sqrt(total / float(entries))
    clip = 1.0 / jnp.maximum(1.0, rms_value / CLIP_RMS)
    q_first, q_second, q_dir = moments(query_first, query_second, query_low, clip)
    k_first, k_second, k_dir = moments(key_first, key_second, key_low, clip)
    b_first, b_second, b_dir = moments(branch_first, branch_second, branch_low, clip)
    step_rows_query = lax.dynamic_slice_in_dim(query_basis, row_index * rows_in, rows_in, 0).astype(
        jnp.float32
    )
    step_rows_key = lax.dynamic_slice_in_dim(key_basis, row_index * rows_in, rows_in, 0).astype(
        jnp.float32
    )
    query_step = jnp.dot(step_rows_query, q_dir, precision=exact)
    key_step = jnp.dot(step_rows_key, k_dir, precision=exact)
    branch_step = jnp.dot(b_dir, own_branch.T, precision=exact)
    query_updated = query_master - LEARN * query_step
    key_updated = key_master - LEARN * key_step
    branch_updated = branch_master - LEARN * branch_step
    query_copy, key_copy, branch_copy = in_one_piece(
        (
            query_updated.astype(jnp.bfloat16),
            key_updated.astype(jnp.bfloat16),
            branch_updated.astype(jnp.bfloat16),
        ),
        FS,
        0,
        1,
    )
    return (
        query_step,
        key_step,
        branch_step,
        query_updated,
        key_updated,
        branch_updated,
        query_copy,
        key_copy,
        branch_copy,
        q_first,
        q_second,
        k_first,
        k_second,
        b_first,
        b_second,
    )


def solution(mesh):
    finer = Mesh(mesh.devices.reshape(4, 4, 8, 2), ("fs_0", "fs_1", "tp_0", "tp_1"))
    return jax.shard_map(
        per_device,
        mesh=finer,
        in_specs=(
            P(FS, TP),
            P(FS, TP),
            P(FS, TP),
            P(FS, TP),
            P(FS, TP),
            P(FS, TP),
            P(FS, TP),
            P(FS, TP),
            P(),
            P(),
            P(),
            P(None, TP),
            P(None, TP),
            P(None, TP),
            P(None, TP),
            P(FS, None),
            P(FS, None),
        ),
        out_specs=(
            P(FS, TP),
            P(FS, TP),
            P(FS, TP),
            P(FS, TP),
            P(FS, TP),
            P(FS, TP),
            P(None, TP),
            P(None, TP),
            P(None, TP),
            P(None, TP),
            P(None, TP),
            P(None, TP),
            P(None, TP),
            P(FS, None),
            P(FS, None),
        ),
        check_vma=False,
    )
```

profile of v0, /device:TPU:32, one launch (start us, length us, event | category | flops | bytes accessed | tf_op | source)
XLA Modules:
  0.0 396.6 jit_solution(3107865244808029063)
XLA Ops:
  7.2 0.7 all-gather.5.cloned.1.call-update
  7.9 1.4 convolution_bitcast_fusion
  9.3 67.5 %all-gather.5.cloned.1.call-done = bf16[1024,4096]{1,0:T(8,128)(2,1)} async-done(((bf16[1024,256]{1,0:T(8,128)(2,1)}), bf16[1024,4096]{1,0:T(8,128)(2,1)}) %all-gather.5.cloned.1.call-update) | async-done | bytes 8388624 | tf_op jit(solution)/shard_map/all_gather | solution.py:125
  76.8 7.8 %fusion.39 = f32[4096,256]{1,0:T(8,128)} fusion(bf16[1024,4096]{1,0:T(8,128)(2,1)} %all-gather.5.cloned.1.call-done, bf16[1024,256]{1,0:T(8,128)(2,1)} %param.21), kind=kOutput, calls=%fused_computation.61 | convolution fusion | flops 2147483648 | bytes 13107200 | tf_op jit(solution)/shard_map/dot_general | solution.py:87
  84.6 6.2 %all-to-all-start.1 = ((f32[16,256,256]{2,1,0:T(8,128)}), f32[16,256,256]{2,1,0:T(8,128)}, u32[]{:S(2)}, u32[]{:S(2)}) async-start(f32[16,256,256]{2,1,0:T(8,128)} %bitcast.24), calls=%async_computation.1 | async-start | bytes 8388608 | tf_op jit(solution)/shard_map/all_to_all | solution.py:38
  91.0 0.3 convolution_bitcast_fusion.1
  91.3 0.2 copy.71
  91.5 0.2 copy.70
  91.7 1.0 pad_maximum_fusion
  92.8 61.8 %all-to-all-done.1 = f32[16,256,256]{2,1,0:T(8,128)} async-done(((f32[16,256,256]{2,1,0:T(8,128)}), f32[16,256,256]{2,1,0:T(8,128)}, u32[]{:S(2)}, u32[]{:S(2)}) %all-to-all-start.1) | async-done | bytes 4194336 | tf_op jit(solution)/shard_map/all_to_all | solution.py:38
  154.6 2.5 reduce_sum.57
  157.1 1.8 fusion.23
  158.9 46.4 %all-reduce.2.cloned.1.call-done = f32[262144]{0:T(1024)} async-done(((f32[262144]{0:T(1024)}), f32[262144]{0:T(1024)}) %all-reduce.2.cloned.1.call-update) | async-done | bytes 1048592 | tf_op jit(solution)/shard_map/psum | solution.py:23
  205.3 1.6 fusion
  206.9 0.1 reshape.96
  207.0 1.6 convolution_bitcast_fusion.2
  208.8 3.5 broadcast_in_dim.2
  212.3 7.0 %all-to-all-start = ((f32[16,1,40960]{2,1,0:T(1,128)}), f32[16,1,40960]{2,1,0:T(1,128)}, u32[]{:S(2)}, u32[]{:S(2)}) async-start(f32[16,1,40960]{2,1,0:T(1,128)} %broadcast_in_dim.2), calls=%async_computation | async-start | bytes 5242880 | tf_op jit(solution)/shard_map/all_to_all | solution.py:44
  219.4 0.1 copy.74
  219.5 40.6 %all-to-all-done = f32[16,1,40960]{2,1,0:T(1,128)} async-done(((f32[16,1,40960]{2,1,0:T(1,128)}), f32[16,1,40960]{2,1,0:T(1,128)}, u32[]{:S(2)}, u32[]{:S(2)}) %all-to-all-start) | async-done | bytes 2621472 | tf_op jit(solution)/shard_map/all_to_all | solution.py:44
  260.1 3.4 reduce_sum.54
  263.6 0.6 multiply_reduce_fusion.2
  264.2 0.6 multiply_reduce_fusion.1
  266.1 1.7 reduce_sum.58
  267.8 0.6 multiply_reduce_fusion
  269.1 0.1 copy.75
  269.2 10.0 %psum.36 = f32[]{:T(128)} all-reduce(f32[]{:T(128)S(6)} %add.73), channel_id=1, replica_groups=mesh['fs_0'=4,'fs_1'=4,'tp_0'=8,'tp_1'=2] {'fs_0'}, use_global_device_ids=true, to_apply=%region_7.0 | all-reduce | flops 1 | bytes 8 | tf_op jit(solution)/shard_map/psum | solution.py:67
  279.2 0.1 copy.76
  279.4 8.4 %psum.37 = f32[]{:T(128)} all-reduce(f32[]{:T(128)} %psum.36), channel_id=1, replica_groups=mesh['fs_0'=4,'fs_1'=4,'tp_0'=8,'tp_1'=2] {'fs_1'}, use_global_device_ids=true, to_apply=%region_8.0 | all-reduce | flops 1 | bytes 8 | tf_op jit(solution)/shard_map/psum | solution.py:67
  287.7 0.1 copy.77
  287.9 18.6 %psum.38 = f32[]{:T(128)} all-reduce(f32[]{:T(128)} %psum.37), channel_id=1, replica_groups=mesh['fs_0'=4,'fs_1'=4,'tp_0'=8,'tp_1'=2] {'tp_0'}, use_global_device_ids=true, to_apply=%region_9.0 | all-reduce | flops 1 | bytes 8 | tf_op jit(solution)/shard_map/psum | solution.py:67
  306.5 3.3 psum.39
  310.6 0.1 mul.166
  310.9 1.8 fusion.36
  312.7 0.3 fusion.35
  313.1 1.2 fusion.37
  314.2 0.7 pad_maximum_fusion.1
  315.0 0.7 copy.85
  315.7 0.7 copy.84
  316.4 0.8 copy.80
  317.2 0.8 copy.78
  318.1 0.8 copy.81
  318.9 0.8 copy.79
  319.7 58.0 %all-gather.7.cloned.1.call-done = bf16[4096,576]{0,1:T(8,128)(2,1)} async-done(((bf16[256,576]{0,1:T(8,128)(2,1)}), bf16[4096,576]{0,1:T(8,128)(2,1)}) %all-gather.7.cloned.1.call-update) | async-done | bytes 4718608 | tf_op jit(solution)/shard_map/all_gather | solution.py:76
  377.7 3.9 fusion.38
  381.7 4.1 %copy.83 = bf16[4096,256]{1,0:T(8,128)(2,1)} copy(bf16[4096,256]{0,1:T(8,128)(2,1)} %get-tuple-element.81) | data formatting | bytes 4194304
  385.7 2.4 copy.82
  388.2 1.9 split.13
  (50 shorter events, 0.6 us)
Async XLA Ops:
  7.2 83.8 %copy-start = (bf16[4096,128]{1,0:T(8,128)(2,1)S(1)}, bf16[4096,128]{1,0:T(8,128)(2,1)}, u32[]{:S(2)}) copy-start(bf16[4096,128]{1,0:T(8,128)(2,1)} %param.25) | copy-start | bytes 3145732
  7.2 69.6 %all-gather.5.cloned.1.call-start = ((), (), s32[]{:S(2)}) async-start(), calls=%async_computation.3 | async-start | bytes 8912896 | tf_op jit(solution)/shard_map/all_gather | solution.py:125
  84.6 6.3 %copy-start.1 = (bf16[1024,256]{1,0:T(8,128)(2,1)S(1)}, bf16[1024,256]{1,0:T(8,128)(2,1)}, u32[]{:S(2)}) copy-start(bf16[1024,256]{1,0:T(8,128)(2,1)} %param.17) | copy-start | bytes 1572868
  84.6 70.0 %all-to-all-start.1 = ((f32[16,256,256]{2,1,0:T(8,128)}), f32[16,256,256]{2,1,0:T(8,128)}, u32[]{:S(2)}, u32[]{:S(2)}) async-start(f32[16,256,256]{2,1,0:T(8,128)} %bitcast.24), calls=%async_computation.1 | async-start | bytes 8388608 | tf_op jit(solution)/shard_map/all_to_all | solution.py:38
  90.9 114.4 %all-reduce.2.cloned.1.call-start = ((), (), s32[]{:S(2)}) async-start(), calls=%async_computation.2 | async-start | bytes 2097152 | tf_op jit(solution)/shard_map/psum | solution.py:23
  91.7 113.6 %copy-start.11 = (bf16[1024,64]{0,1:T(8,128)(2,1)S(1)}, bf16[1024,64]{0,1:T(8,128)(2,1)}, u32[]{:S(2)}) copy-start(bf16[1024,64]{0,1:T(8,128)(2,1)} %param.19) | copy-start | bytes 393220
  91.7 115.3 %copy-start.4 = (bf16[1024,256]{1,0:T(8,128)(2,1)S(1)}, bf16[1024,256]{1,0:T(8,128)(2,1)}, u32[]{:S(2)}) copy-start(bf16[1024,256]{1,0:T(8,128)(2,1)} %param.18) | copy-start | bytes 1572868
  92.8 173.3 %all-gather.9.cloned.1.call-start = ((), (), s32[]{:S(2)}) async-start(), calls=%async_computation.5 | async-start | bytes 2228224 | tf_op jit(solution)/shard_map/all_gather | solution.py:62
  208.7 10.7 %copy-start.15 = (f32[128,64]{0,1:T(8,128)S(1)}, f32[128,64]{0,1:T(8,128)}, u32[]{:S(2)}) copy-start(f32[128,64]{0,1:T(8,128)} %param.30) | copy-start | bytes 98308
  212.3 56.8 %copy-start.16 = (f32[128,64]{0,1:T(8,128)S(1)}, f32[128,64]{0,1:T(8,128)}, u32[]{:S(2)}) copy-start(f32[128,64]{0,1:T(8,128)} %param.31) | copy-start | bytes 98308
  212.3 66.9 %copy-start.7 = (f32[256,256]{1,0:T(8,128)S(1)}, f32[256,256]{1,0:T(8,128)}, u32[]{:S(2)}) copy-start(f32[256,256]{1,0:T(8,128)} %param.22) | copy-start | bytes 786436
  212.3 47.8 %all-to-all-start = ((f32[16,1,40960]{2,1,0:T(1,128)}), f32[16,1,40960]{2,1,0:T(1,128)}, u32[]{:S(2)}, u32[]{:S(2)}) async-start(f32[16,1,40960]{2,1,0:T(1,128)} %broadcast_in_dim.2), calls=%async_computation | async-start | bytes 5242880 | tf_op jit(solution)/shard_map/all_to_all | solution.py:44
  219.3 68.4 %copy-start.8 = (f32[256,256]{1,0:T(8,128)S(1)}, f32[256,256]{1,0:T(8,128)}, u32[]{:S(2)}) copy-start(f32[256,256]{1,0:T(8,128)} %param.24) | copy-start | bytes 786436
  219.3 91.4 %copy-start.12 = (f32[256,128]{1,0:T(8,128)S(1)}, f32[256,128]{1,0:T(8,128)}, u32[]{:S(2)}) copy-start(f32[256,128]{1,0:T(8,128)} %param.33) | copy-start | bytes 393220
  219.3 91.4 %copy-start.13 = (f32[256,128]{1,0:T(8,128)S(1)}, f32[256,128]{1,0:T(8,128)}, u32[]{:S(2)}) copy-start(f32[256,128]{1,0:T(8,128)} %param.32) | copy-start | bytes 393220
  219.3 91.5 %copy-start.9 = (f32[128,256]{1,0:T(8,128)S(1)}, f32[128,256]{1,0:T(8,128)}, u32[]{:S(2)}) copy-start(f32[128,256]{1,0:T(8,128)} %param.29) | copy-start | bytes 393220
  219.3 91.5 %copy-start.10 = (f32[128,256]{1,0:T(8,128)S(1)}, f32[128,256]{1,0:T(8,128)}, u32[]{:S(2)}) copy-start(f32[128,256]{1,0:T(8,128)} %param.28) | copy-start | bytes 393220
  219.4 158.4 %all-gather.7.cloned.1.call-start = ((), (), s32[]{:S(2)}) async-start(), calls=%async_computation.4 | async-start | bytes 5013504 | tf_op jit(solution)/shard_map/all_gather | solution.py:76
  219.5 91.4 %copy-start.14 = (f32[256,64]{0,1:T(8,128)S(1)}, f32[256,64]{0,1:T(8,128)}, u32[]{:S(2)}) copy-start(f32[256,64]{0,1:T(8,128)} %param.23) | copy-start | bytes 196612
  310.7 9.0 %copy-start.6 = (f32[256,128]{1,0:T(8,128)}, f32[256,128]{1,0:T(8,128)S(1)}, u32[]{:S(2)}) copy-start(f32[256,128]{1,0:T(8,128)S(1)} %get-tuple-element.84) | copy-start | bytes 393220
  310.7 70.9 %copy-start.5 = (f32[256,128]{1,0:T(8,128)}, f32[256,128]{1,0:T(8,128)S(1)}, u32[]{:S(2)}) copy-start(f32[256,128]{1,0:T(8,128)S(1)} %get-tuple-element.83) | copy-start | bytes 393220
  310.9 70.8 %copy-start.2 = (f32[128,256]{1,0:T(8,128)}, f32[128,256]{1,0:T(8,128)S(1)}, u32[]{:S(2)}) copy-start(f32[128,256]{1,0:T(8,128)S(1)} %get-tuple-element.85) | copy-start | bytes 393220
  310.9 70.8 %copy-start.3 = (f32[128,256]{1,0:T(8,128)}, f32[128,256]{1,0:T(8,128)S(1)}, u32[]{:S(2)}) copy-start(f32[128,256]{1,0:T(8,128)S(1)} %get-tuple-element.86) | copy-start | bytes 393220
Sparse Core Ops, SparseCore 0:
  9.8 67.0 all-gather.4
  94.6 110.6 all-reduce.1
  207.7 42.0 all-gather.8
  315.1 62.5 all-gather.6
where the time goes:
time: 397 us
  waiting for transfers between devices  275 us (69%)
  blocking collectives  40.3 us (10%)
  local copies, waits for them, and re-layouts  21.8 us (5%)
  matrix products  17.9 us (5%)
  between operations  16.8 us (4%)
  starting transfers between devices  13.4 us (3%)
  other arithmetic  11.4 us (3%)
    all_gather x1, waiting for transfers between devices, per_device(): whole_values = lax.all_gather(head_outputs, TP, axis=1, tiled=True)  67.5 us
    all_to_all x1, waiting for transfers between devices, sum_at_owner(): lax.all_to_all(pieces, axis, split_axis=0, concat_axis=0, tiled=True)  61.8 us
    all_gather x1, waiting for transfers between devices, in_one_piece(): lax.all_gather(both, axis, axis=dim, tiled=True)  58 us
    psum x1, waiting for transfers between devices, together(): subtotal = lax.psum(vector, axis)  46.4 us
    all_to_all x1, waiting for transfers between devices, copy_for_each(): lax.all_to_all(jnp.broadcast_to(array[None], (length, *array.shape)), axi...  40.6 us
    psum x4, blocking collectives, over_axes(): return functools.reduce(lax.psum, axes, array)  40.3 us
    unnamed x47, local copies, waits for them, and re-layouts  11.9 us
    dot_general x3, matrix products, over_tokens(): lax.dot_general(left, right, (((0,), (0,)), ((), ())), precision=precisio...  11.1 us
  transfers between devices with their start and end apart: 6, of which 5 were waited for; matrix products, arithmetic and copies ran while one was open for 6% of the time, Pallas kernels for 0%

commit v1 on v0

v1 whole, which is shorter than its diff:
```python
import functools

import jax
import jax.numpy as jnp
from jax import lax
from jax.experimental import pallas as pl
from jax.experimental.pallas import tpu as pltpu
from jax.sharding import Mesh
from jax.sharding import PartitionSpec as P

FS = ("fs_0", "fs_1")
TP = ("tp_0", "tp_1")
MESH = pl.DeviceIdType.MESH

LEARN = 0.02
BETA_ONE = 0.9
BETA_TWO = 0.95
ADAM_EPS = 1e-08
CLIP_RMS = 0.5

NY, NX, NZ, NC = 4, 4, 8, 2
NF, NT = NY * NX, NZ * NC
F32, BF16 = jnp.float32, jnp.bfloat16
REACH = {(0, 1): 4, (0, -1): 3, (1, 1): 3, (1, -1): 4}
AXES = {"y": "fs_0", "x": "fs_1", "z": "tp_0", "c": "tp_1"}


def dot(a, b, ca=1, cb=0):
    return lax.dot_general(a, b, (((ca,), (cb,)), ((), ())), preferred_element_type=F32)


def split(value):
    high = value.astype(BF16)
    return high, (value - high.astype(F32)).astype(BF16)


def moments(first, second, low, clip):
    scaled = clip * low
    first_new = BETA_ONE * first + (1.0 - BETA_ONE) * scaled
    second_new = BETA_TWO * second + (1.0 - BETA_TWO) * scaled * scaled
    return first_new, second_new, first_new / (jnp.sqrt(second_new) + ADAM_EPS)


class Gather:
    def __init__(self, buf, y, x, send, recv):
        self.buf, self.at, self.send, self.recv = buf, {"y": y, "x": x}, send, recv
        self.half = buf.shape[1] // 2
        self.sent = []

    def copy(self, h, kind, a, way, arriving):
        dims = ("x", "y") if h == 0 else ("y", "x")
        index = {"p1": 0, "f1": 2, "p2": 4, "f2": 12}[kind] + (0 if way == 1 else 1)
        if kind in ("p2", "f2"):
            index += 2 * (0, -1, 1, 2).index(a)
        passed = (0 if kind[0] == "p" else 1) + (1 if arriving else 0)
        off = (-way * passed, 0) if kind[1] == "1" else (a, -way * passed)
        pos = {d: lax.rem(self.at[d] + (o + 4), 4) for d, o in zip(dims, off)}
        block = pos["y"] * NX + pos["x"]
        start, size = h * self.half, self.half
        if kind[0] == "f":
            size //= 2
            start += 0 if way == 1 else size
        ref = self.buf.at[block, pl.ds(start, size)]
        dim = dims[int(kind[1]) - 1]
        return pltpu.make_async_remote_copy(
            src_ref=ref,
            dst_ref=ref,
            send_sem=self.send.at[h * 20 + index],
            recv_sem=self.recv.at[h * 20 + index],
            device_id={AXES[dim]: lax.rem(self.at[dim] + (way + 4), 4)},
            device_id_type=MESH,
        )

    def start(self, h, kind, a, way):
        self.copy(h, kind, a, way, False).start()
        self.sent.append((h, kind, a, way))

    def wait(self, h, kind, a, way):
        self.copy(h, kind, a, way, True).wait_recv()

    def both(self, h, a):
        for way in (1, -1):
            self.start(h, "p2", a, way)

    def step(self, n):
        for h in (0, 1):
            if n == 0:
                for way in (1, -1):
                    self.start(h, "p1", 0, way)
                self.both(h, 0)
            elif n == 1:
                for way in (1, -1):
                    self.wait(h, "p1", 0, way)
                    self.start(h, "f1", 0, way)
                    self.both(h, -way)
            elif n == 3:
                for way in (1, -1):
                    self.wait(h, "f1", 0, way)
                self.both(h, 2)
            elif n == 6:
                for a in (0, -1, 1, 2):
                    for way in (1, -1):
                        self.wait(h, "f2", a, way)
            else:
                for a in {2: (0,), 4: (-1, 1), 5: (2,)}[n]:
                    for way in (1, -1):
                        self.wait(h, "p2", a, way)
                        self.start(h, "f2", a, way)

    def finish(self):
        for m in self.sent:
            self.copy(*m, False).wait_send()


def exchange_kernel(
    x_hbm, uq_hbm, uk_hbm, h_hbm, ub_hbm, mq_hbm, mk_hbm, mb_hbm, bq_hbm, bk_hbm, bb_hbm,
    qf_hbm, qs_hbm, kf_hbm, ks_hbm, bf_hbm, bs_hbm,
    qc_out, kc_out, bc_out, lq_out, lk_out, lb_out, clip_out,
    xv, uv, uqv, ukv, hv, bqv, bkv, bbv, mkv, mbv, qf, qs, kf, ks, bf, bs,
    g, gb, s1, rr, ss, p2, hi, lo, s2, r2, g3, b3, s4, r4, oq, ok, qd, kd,
    lsem, dsend, drecv, zs, zr, as_, ar, fwds, fwdr, g1s, g1r, g2s, g2r, ps, pr, osem,
):
    y, x = lax.axis_index("fs_0"), lax.axis_index("fs_1")
    z, c = lax.axis_index("tp_0"), lax.axis_index("tp_1")
    f, t = y * NX + x, z * NC + c

    loads = []

    def load(src, dst):
        copy = pltpu.make_async_copy(src, dst, lsem.at[len(loads)])
        copy.start()
        loads.append(copy)
        return copy

    mine, other = pl.ds(c * 512, 512), pl.ds((1 - c) * 512, 512)
    gq0 = load(mq_hbm.at[:, pl.ds(0, 128)], g.at[f, pl.ds(0, 256)])
    gq1 = load(mq_hbm.at[:, pl.ds(128, 128)], g.at[f, pl.ds(256, 256)])
    gk = load(mk_hbm, mkv)
    first = [
        load(x_hbm.at[mine], xv.at[c]),
        load(ub_hbm.at[mine], uv.at[c]),
        load(bb_hbm.at[pl.ds(z * 512, 512)], bbv),
        load(bq_hbm, bqv),
        load(bk_hbm, bkv),
    ]
    second = [load(uq_hbm, uqv), load(uk_hbm, ukv), load(h_hbm, hv)]
    third = [
        load(a, b)
        for a, b in (
            (mb_hbm, mbv), (qf_hbm, qf), (qs_hbm, qs), (kf_hbm, kf), (ks_hbm, ks), (bf_hbm, bf), (bs_hbm, bs),
        )
    ]

    def fs_peer(d):
        p = lax.rem(f + d, NF)
        return p, {"fs_0": p // NX, "fs_1": lax.rem(p, NX)}

    def tp_peer(d):
        p = lax.rem(t + d, NT)
        return p, {"tp_0": p // NC, "tp_1": lax.rem(p, NC)}

    barrier = pltpu.get_barrier_semaphore()

    @pl.loop(1, 16)
    def _(d):
        pl.semaphore_signal(barrier, inc=1, device_id=fs_peer(d)[1], device_id_type=MESH)
        pl.semaphore_signal(barrier, inc=1, device_id=tp_peer(d)[1], device_id_type=MESH)

    pl.semaphore_wait(barrier, 30)

    def remote(src, dst, send, recv, to):
        return pltpu.make_async_remote_copy(
            src_ref=src, dst_ref=dst, send_sem=send, recv_sem=recv, device_id=to, device_id_type=MESH
        )

    partner = {"tp_1": 1 - c}
    swaps = [
        remote(x_hbm.at[other], xv.at[c], dsend.at[0], drecv.at[0], partner),
        remote(ub_hbm.at[other], uv.at[c], dsend.at[1], drecv.at[1], partner),
    ]
    for s in swaps:
        s.start()

    gk.wait()
    g[f, pl.ds(512, 128)] = jnp.concatenate([mkv[0:128], mkv[128:256]], axis=1)
    gq0.wait()
    gq1.wait()
    whole = Gather(g, y, x, g1s, g1r)
    whole.step(0)

    for a in first:
        a.wait()
    for s in swaps:
        s.wait_recv()
    za, zb = pl.ds(z * 512, 256), pl.ds(z * 512 + 256, 256)
    proj = (
        dot(xv[0], bqv[za]) + dot(xv[1], bqv[zb]),
        dot(xv[0], bkv[za]) + dot(xv[1], bkv[zb]),
        dot(uv[0], bbv[0:256]) + dot(uv[1], bbv[256:512]),
    )
    for i in range(3):
        for o in range(NZ):
            for h in (0, 1):
                at = (2 * o + h) * 32
                s1[o, h, i * 32 : i * 32 + 32] = proj[i][at : at + 32]

    def ring(table, h, way, s):
        index = (h * 2 + (0 if way == 1 else 1)) * 4 + s
        return table.at[index]

    def zmove(src, dst, sends, recvs, h, way, s):
        to = {"tp_0": lax.rem(z + (way + NZ), NZ)}
        return remote(src, dst, ring(sends, h, way, s), ring(recvs, h, way, s), to)

    lanes = [(h, way) for h in (0, 1) for way in (1, -1)]
    zsent = []
    for s in range(4):
        for h, way in lanes:
            reach = REACH[h, way]
            if s >= reach:
                continue
            owner = lax.rem(z + way * (reach - s) + NZ, NZ)
            if s == 0:
                src = s1.at[owner, h]
            else:
                zmove(src, ring(rr, h, way, s - 1), zs, zr, h, way, s - 1).wait_recv()
                src = ring(ss, h, way, s)
                src[...] = ring(rr, h, way, s - 1)[...] + s1[owner, h]
            zsent.append((src, ring(rr, h, way, s), zs, zr, h, way, s))
            zmove(*zsent[-1]).start()
        if s == 2:
            whole.step(1)
    whole.step(2)
    for h in (0, 1):
        total = s1[z, h]
        for way in (1, -1):
            last = REACH[h, way] - 1
            zmove(s1.at[z, h], ring(rr, h, way, last), zs, zr, h, way, last).wait_recv()
            total = total + ring(rr, h, way, last)[...]
        p2[c, z, h] = total

    def over(h, o, index):
        ref = p2.at[c, o, h]
        return remote(ref, ref, fwds.at[h * 8 + index], fwdr.at[h * 8 + index], partner)

    asent, osent = [], []

    def onward(h, o, index):
        over(h, o, index).start()
        osent.append((h, o, index))

    for s in range(5):
        for h, way in lanes:
            reach = REACH[h, way]
            if s > reach:
                continue
            o = lax.rem(z - way * s + NZ, NZ)
            ref = p2.at[c, o, h]
            if s > 0:
                zmove(ref, ref, as_, ar, h, way, s - 1).wait_recv()
            if s < reach:
                zmove(ref, ref, as_, ar, h, way, s).start()
                asent.append((ref, ref, as_, ar, h, way, s))
            if s > 0 or way == 1:
                onward(h, o, s if way == 1 else NZ - s)
        if s == 1:
            whole.step(3)
        if s == 3:
            whole.step(4)

    for a in second:
        a.wait()

    def spread(half):
        for i in range(3):
            value = p2[half, :, :, i * 32 : i * 32 + 32].reshape(512, 128)
            rows = pl.ds(half * 512, 512)
            hi[i, rows], lo[i, rows] = split(value)

    spread(c)
    for h in (0, 1):
        for index in range(NZ):
            o = lax.rem(z - index + NZ, NZ)
            ref = p2.at[1 - c, o, h]
            remote(ref, ref, fwds.at[h * 8 + index], fwdr.at[h * 8 + index], partner).wait_recv()
    spread(1 - c)

    uq, uk, hh = uqv[...], ukv[...], hv[...]
    low_q = dot(hi[0], uq, 0, 0) + dot(lo[0], uq, 0, 0)
    low_k = dot(hi[1], uk, 0, 0) + dot(lo[1], uk, 0, 0)
    low_b = dot(hh, hi[2], 0, 0) + dot(hh, lo[2], 0, 0)
    low_k = jnp.concatenate([low_k, jnp.zeros((128, 64), F32)], axis=1)
    for p in range(NF):
        s2[p, 0:8] = low_q[8 * p : 8 * p + 8, 0:128]
        s2[p, 8:16] = low_q[8 * p : 8 * p + 8, 128:256]
        s2[p, 16:24] = low_k[8 * p : 8 * p + 8]
        s2[p, 24:40] = low_b[16 * p : 16 * p + 16]

    def fs_all(src, dst, k, act):
        @pl.loop(1, 16)
        def _(d):
            p, to = fs_peer(d)
            act(remote(src(p), dst.at[f], ps.at[k, d], pr.at[k, d], to))

    def tp_all(src, dst, k, act):
        @pl.loop(1, 16)
        def _(d):
            _, to = tp_peer(d)
            act(remote(src, dst.at[t], ps.at[k, d], pr.at[k, d], to))

    def fs_arrive(dst, k):
        @pl.loop(1, 16)
        def _(d):
            p = lax.rem(f + NF - d, NF)
            remote(dst.at[p], dst.at[p], ps.at[k, d], pr.at[k, d], fs_peer(d)[1]).wait_recv()

    def tp_arrive(dst, k):
        @pl.loop(1, 16)
        def _(d):
            p = lax.rem(t + NT - d, NT)
            remote(dst.at[p], dst.at[p], ps.at[k, d], pr.at[k, d], tp_peer(d)[1]).wait_recv()

    begin = lambda m: m.start()
    left = lambda m: m.wait_send()
    fs_all(lambda p: s2.at[p], r2, 0, begin)
    r2[f] = s2[f]
    fs_arrive(r2, 0)
    piece = r2[0]
    for p in range(1, NF):
        piece = piece + r2[p]
    squares = piece * piece
    tile = squares[0:8]
    for i in range(1, 5):
        tile = tile + squares[8 * i : 8 * i + 8]
    b3[t, 0:16] = piece[24:40]
    b3[t, 16:24] = tile
    g3[f] = piece[0:24]
    tp_all(b3.at[t], b3, 1, begin)
    fs_all(lambda p: g3.at[f], g3, 2, begin)
    tp_arrive(b3, 1)
    tile = b3[0, 16:24]
    for i in range(1, NT):
        tile = tile + b3[i, 16:24]
    for i in range(NT):
        s4[i, 0:16] = b3[i, 0:16]
        s4[i, 16:24] = tile
    fs_all(lambda p: s4.at[p], r4, 3, begin)
    r4[f] = s4[f]
    fs_arrive(g3, 2)
    whole.step(5)
    fs_arrive(r4, 3)
    tile = r4[0, 16:24]
    for i in range(1, NF):
        tile = tile + r4[i, 16:24]
    total = jnp.sum(jnp.sum(tile, axis=0, keepdims=True), axis=1, keepdims=True)
    entries = 128 * (2 * 4096 + 1024)
    rms = jnp.sqrt(total / float(entries))
    clip = 1.0 / jnp.maximum(1.0, rms / CLIP_RMS)
    clip_out[...] = jnp.broadcast_to(clip, (8, 128))

    for a in third:
        a.wait()

    low_b = r4[:, 0:16].reshape(256, 128)
    lb_out[...] = low_b
    _, _, dir_b = moments(bf[...], bs[...], low_b, clip)
    dh, dl = split(dir_b)
    cols = bbv[pl.ds(c * 256, 256)]
    new_b = (mbv[...] - LEARN * (dot(dh, cols, 1, 1) + dot(dl, cols, 1, 1))).astype(BF16)
    gb[f, 0:256] = new_b[:, 0:128]
    gb[f, 256:512] = new_b[:, 128:256]
    branch = Gather(gb, y, x, g2s, g2r)
    branch.step(0)

    low_q = jnp.concatenate([g3[:, 0:8].reshape(128, 128), g3[:, 8:16].reshape(128, 128)], axis=1)
    low_k = g3[:, 16:24].reshape(128, 128)[:, 0:64]
    lq_out[...] = low_q
    lk_out[...] = low_k
    _, _, dir_q = moments(qf[...], qs[...], low_q, clip)
    _, _, dir_k = moments(kf[...], ks[...], low_k, clip)
    qd[0], qd[1] = split(dir_q)
    kd[0], kd[1] = split(dir_k)
    whole.step(6)

    def own_columns(j):
        rows = pl.ds(pl.multiple_of(j * 256, 256), 256)
        bq, bk = bqv[rows], bkv[rows]
        step = LEARN * (dot(bq, qd[0]) + dot(bq, qd[1]))
        oq[rows, 0:128] = (g[j, 0:256] - step[:, 0:128]).astype(BF16)
        oq[rows, 128:256] = (g[j, 256:512] - step[:, 128:256]).astype(BF16)
        step = LEARN * (dot(bk, kd[0]) + dot(bk, kd[1]))
        pair = g[j, 512:640]
        ok[rows] = (jnp.concatenate([pair[:, 0:64], pair[:, 64:128]], axis=0) - step).astype(BF16)

    def put(j, act):
        rows = pl.ds(pl.multiple_of(j * 1024, 1024), 1024)
        act(pltpu.make_async_copy(oq.at[rows], qc_out.at[rows], osem.at[0, j]))
        act(pltpu.make_async_copy(ok.at[rows], kc_out.at[rows], osem.at[1, j]))

    for quarter in range(4):
        pl.loop(quarter * 4, quarter * 4 + 4)(own_columns)
        put(quarter, begin)
        branch.step(quarter + 1)
    branch.step(5)
    branch.step(6)

    def put_branch(act):
        @pl.loop(0, 16)
        def _(j):
            rows = pl.ds(pl.multiple_of(j * 256, 256), 256)
            for half in (0, 1):
                src = gb.at[j, pl.ds(half * 256, 256)]
                act(pltpu.make_async_copy(src, bc_out.at[rows, pl.ds(half * 128, 128)], osem.at[2 + half, j]))

    put_branch(begin)

    for s in swaps:
        s.wait_send()
    for m in zsent + asent:
        zmove(*m).wait_send()
    for m in osent:
        over(*m).wait_send()
    fs_all(lambda p: s2.at[p], r2, 0, left)
    tp_all(b3.at[t], b3, 1, left)
    fs_all(lambda p: g3.at[f], g3, 2, left)
    fs_all(lambda p: s4.at[p], r4, 3, left)
    whole.finish()
    branch.finish()
    for quarter in range(4):
        put(quarter, lambda m: m.wait())
    put_branch(lambda m: m.wait())


def finish_kernel(
    mq, mk, mb, bq, bk, bb, qf, qs, kf, ks, bf, bs, lq, lk, lb, clip_ref,
    q_step, k_step, b_step, q_new, k_new, b_new, qf_new, qs_new, kf_new, ks_new, bf_new, bs_new,
    bqv, bkv, bbv, sem,
):
    f = lax.axis_index("fs_0") * NX + lax.axis_index("fs_1")
    t = lax.axis_index("tp_0") * NC + lax.axis_index("tp_1")
    copies = [
        pltpu.make_async_copy(src.at[pl.ds(at * 256, 256)], dst, sem.at[i])
        for i, (src, dst, at) in enumerate(((bq, bqv, f), (bk, bkv, f), (bb, bbv, t)))
    ]
    for copy in copies:
        copy.start()
    clip = clip_ref[0:1, 0:1]
    for copy in copies:
        copy.wait()

    def one(first, second, low, master, basis, first_out, second_out, step_out, new_out, branch):
        first_out[...], second_out[...], way = moments(first[...], second[...], low[...], clip)
        high, rest = split(way)
        if branch:
            step = dot(high, basis[...], 1, 1) + dot(rest, basis[...], 1, 1)
        else:
            step = dot(basis[...], high) + dot(basis[...], rest)
        step_out[...] = step
        new_out[...] = master[...] - LEARN * step

    one(qf, qs, lq, mq, bqv, qf_new, qs_new, q_step, q_new, False)
    one(kf, ks, lk, mk, bkv, kf_new, ks_new, k_step, k_new, False)
    one(bf, bs, lb, mb, bbv, bf_new, bs_new, b_step, b_new, True)


def per_device(*args):
    (_, _, _, _, _, mq, mk, mb, bq, bk, bb, qf, qs, kf, ks, bf, bs) = args
    shape = jax.ShapeDtypeStruct
    hbm = pl.BlockSpec(memory_space=pl.ANY)
    vmem = pl.BlockSpec(memory_space=pltpu.VMEM)
    v, dma = pltpu.VMEM, pltpu.SemaphoreType.DMA
    qc, kc, bc, lq, lk, lb, clip = pl.pallas_call(
        exchange_kernel,
        name="exchange",
        out_shape=(
            shape((4096, 256), BF16),
            shape((4096, 64), BF16),
            shape((4096, 256), BF16),
            shape((128, 256), F32),
            shape((128, 64), F32),
            shape((256, 128), F32),
            shape((8, 128), F32),
        ),
        in_specs=[hbm] * 17,
        out_specs=(hbm, hbm, hbm, vmem, vmem, vmem, vmem),
        scratch_shapes=[
            v((2, 512, 256), BF16), v((2, 512, 256), BF16), v((1024, 256), BF16), v((1024, 64), BF16),
            v((1024, 256), BF16), v((4096, 128), BF16), v((4096, 128), BF16), v((512, 128), BF16),
            v((256, 64), F32), v((256, 256), F32), v((128, 256), F32), v((128, 256), F32),
            v((128, 64), F32), v((128, 64), F32), v((256, 128), F32), v((256, 128), F32),
            v((16, 640, 128), F32), v((16, 512, 128), BF16), v((8, 2, 96, 128), F32),
            v((16, 96, 128), F32), v((16, 96, 128), F32), v((2, 8, 2, 96, 128), F32),
            v((3, 1024, 128), BF16), v((3, 1024, 128), BF16), v((16, 40, 128), F32), v((16, 40, 128), F32),
            v((16, 24, 128), F32), v((16, 24, 128), F32), v((16, 24, 128), F32), v((16, 24, 128), F32),
            v((4096, 256), BF16), v((4096, 64), BF16), v((2, 128, 256), BF16), v((2, 128, 64), BF16),
            dma((18,)), dma((2,)), dma((2,)), dma((16,)), dma((16,)), dma((16,)), dma((16,)),
            dma((16,)), dma((16,)), dma((40,)), dma((40,)), dma((40,)), dma((40,)),
            dma((4, 16)), dma((4, 16)), dma((4, 16)),
        ],
        compiler_params=pltpu.CompilerParams(
            collective_id=0, has_side_effects=True, vmem_limit_bytes=56 * 2**20
        ),
    )(*args)
    qst, kst, bst, qu, ku, bu, qf2, qs2, kf2, ks2, bf2, bs2 = pl.pallas_call(
        finish_kernel,
        name="finish",
        out_shape=tuple(
            shape(a.shape, F32) for a in (mq, mk, mb, mq, mk, mb, qf, qs, kf, ks, bf, bs)
        ),
        in_specs=[vmem] * 3 + [hbm] * 3 + [vmem] * 10,
        out_specs=(vmem,) * 12,
        scratch_shapes=[v((256, 128), BF16)] * 3 + [dma((3,))],
    )(mq, mk, mb, bq, bk, bb, qf, qs, kf, ks, bf, bs, lq, lk, lb, clip)
    return (qst, kst, bst, qu, ku, bu, qc, kc, bc, qf2, qs2, kf2, ks2, bf2, bs2)


def solution(mesh):
    finer = Mesh(mesh.devices.reshape(NY, NX, NZ, NC), FS + TP)
    fs_tp, cols, rows = P(FS, TP), P(None, TP), P(FS, None)
    return jax.shard_map(
        per_device,
        mesh=finer,
        in_specs=(fs_tp,) * 8 + (P(),) * 3 + (cols,) * 4 + (rows,) * 2,
        out_specs=(fs_tp,) * 6 + (cols,) * 7 + (rows,) * 2,
        check_vma=False,
    )
```

time: 397 us -> 110 us (0.28)
  waiting for transfers between devices: 275 us -> 0 us
  Pallas kernels: 0 us -> 89.6 us
  blocking collectives: 40.3 us -> 0 us
  matrix products: 17.9 us -> 0 us
  between operations: 16.8 us -> 0.67 us
  starting transfers between devices: 13.4 us -> 0 us
  other arithmetic: 11.4 us -> 0 us
    all_gather x3 -> x0, waiting for transfers between devices: 125 us -> none  [the longest x1 67.5 us: per_device(): whole_values = lax.all_gather(head_outputs, TP, axis=1, tiled=True)]
    all_to_all x2 -> x0, waiting for transfers between devices: 102 us -> none  [the longest x1 61.8 us: sum_at_owner(): lax.all_to_all(pieces, axis, split_axis=0, concat_axis=0, tiled=True)]
    pallas_call x0 -> x2, Pallas kernels: none -> 89.6 us  [the longest x1 85.6 us: per_device(): pl.pallas_call(exchange_kernel, name='exchange', out_shape=(shape((4096,...]
    psum x1 -> x0, waiting for transfers between devices: 46.4 us -> none  [together(): subtotal = lax.psum(vector, axis)]
    psum x4 -> x0, blocking collectives: 40.3 us -> none  [over_axes(): return functools.reduce(lax.psum, axes, array)]
    dot_general x9 -> x0, matrix products: 17.9 us -> none  [the longest x3 11.1 us: over_tokens(): lax.dot_general(left, right, (((0,), (0,)), ((), ())), precision=precisio...]
    all_to_all x2 -> x0, starting transfers between devices: 13.2 us -> none  [the longest x1 6.99 us: copy_for_each(): lax.all_to_all(jnp.broadcast_to(array[None], (length, *array.shape)), axi...]
    reduce_sum x6 -> x0, other arithmetic: 9.49 us -> none  [the longest x1 3.44 us: of_everyone(): return copy_for_each(array, axis).sum(axis=0)]
  transfers between devices with their start and end apart: 6 -> 0, of which waited for: 5 -> 0; matrix products, arithmetic and copies ran while one was open for 6% -> 0% of each run, Pallas kernels for 0% -> 0%
where the time goes in v1:
time: 110 us; the launch traced here: 109 us
  Pallas kernels  89.6 us (81%)
  local copies, waits for them, and re-layouts  18.6 us (17%)
    pallas_call x1, Pallas kernels, per_device(): pl.pallas_call(exchange_kernel, name='exchange', out_shape=(shape((4096,...  85.6 us
    unnamed x15, local copies, waits for them, and re-layouts  18.6 us
    pallas_call x1, Pallas kernels, per_device(): pl.pallas_call(finish_kernel, name='finish', out_shape=tuple((shape(a.sha...  4.02 us

profile of v1, /device:TPU:32, one launch (start us, length us, event | category | flops | bytes accessed | tf_op | source)
XLA Modules:
  0.0 108.9 jit_solution(2468025760881972165)
XLA Ops:
  0.6 1.5 %copy.37.kf_hbm.kf = f32[128,64]{1,0:T(8,128)} copy(f32[128,64]{0,1:T(8,128)} %param.30) | data formatting | bytes 65536 | tf_op args[13]
  2.1 1.5 %copy.38.ks_hbm.ks = f32[128,64]{1,0:T(8,128)} copy(f32[128,64]{0,1:T(8,128)} %param.31) | data formatting | bytes 65536 | tf_op args[14]
  3.6 1.6 %copy.36.mk_hbm.mk = f32[256,64]{1,0:T(8,128)} copy(f32[256,64]{0,1:T(8,128)} %param.23) | data formatting | bytes 131072 | tf_op args[6]
  5.2 1.7 %copy.32.uk_hbm = bf16[1024,64]{1,0:T(8,128)(2,1)} copy(bf16[1024,64]{0,1:T(8,128)(2,1)} %param.19) | data formatting | bytes 262144 | tf_op args[2]
  7.0 85.6 %exchange.1 = (bf16[4096,256]{1,0:T(8,128)(2,1)}, bf16[4096,64]{1,0:T(8,128)(2,1)}, bf16[4096,256]{1,0:T(8,128)(2,1)}, f32[128,256]{1,0:T(8,128)}, f32[128,64]{1...) custom-call(bf16[1024,256]{1,0:T(8,128)(2,1)} %x_hbm.1, bf16[1024,256]{1,0:T(8,128)(2,1)} %uq_hbm.1, ...), custom_call_target="tpu_custom_call" | custom-call | tf_op jit(solution)/shard_map/exchange/pallas_call | solution.py:472
  92.6 2.3 %copy.41 = bf16[4096,64]{0,1:T(8,128)(2,1)} copy(bf16[4096,64]{1,0:T(8,128)(2,1)} %get-tuple-element.60) | data formatting | bytes 1048576
  94.9 0.0 copy-start.1
  94.9 4.0 %finish.1 = (f32[256,256]{1,0:T(8,128)}, f32[256,64]{1,0:T(8,128)}, f32[256,256]{1,0:T(8,128)}, f32[256,256]{1,0:T(8,128)}, f32[256,64]{1,0:T(8,128)}, /*index=5...) custom-call(f32[256,256]{1,0:T(8,128)} %mq.1, ...), custom_call_target="tpu_custom_call" | custom-call | tf_op jit(solution)/shard_map/finish/pallas_call | solution.py:504
  98.9 1.5 %copy.42 = f32[128,64]{0,1:T(8,128)} copy(f32[128,64]{1,0:T(8,128)} %get-tuple-element.64) | data formatting | bytes 65536
  100.5 1.5 %copy.43 = f32[128,64]{0,1:T(8,128)} copy(f32[128,64]{1,0:T(8,128)} %get-tuple-element.65) | data formatting | bytes 65536
  102.0 1.6 %copy.39 = f32[256,64]{0,1:T(8,128)} copy(f32[256,64]{1,0:T(8,128)} %get-tuple-element.54) | data formatting | bytes 131072
  103.6 1.6 %copy.40 = f32[256,64]{0,1:T(8,128)} copy(f32[256,64]{1,0:T(8,128)} %get-tuple-element.57) | data formatting | bytes 131072
  105.2 0.0 copy-done.1
  105.2 0.0 copy-start
  105.3 1.3 %copy.46 = bf16[4096,256]{1,0:T(8,128)(2,1)} copy(bf16[4096,256]{1,0:T(8,128)(2,1)S(1)} %copy-done.1) | data formatting | bytes 4194304
  106.6 1.0 copy-done
  107.6 1.3 %copy.47 = bf16[4096,256]{1,0:T(8,128)(2,1)} copy(bf16[4096,256]{1,0:T(8,128)(2,1)S(1)} %copy-done) | data formatting | bytes 4194304
Async XLA Ops:
  94.9 10.3 %copy-start.1 = (bf16[4096,256]{1,0:T(8,128)(2,1)S(1)}, bf16[4096,256]{1,0:T(8,128)(2,1)}, u32[]{:S(2)}) copy-start(bf16[4096,256]{1,0:T(8,128)(2,1)} %get-tuple-element.89) | copy-start | bytes 6291460
  105.2 2.3 %copy-start = (bf16[4096,256]{1,0:T(8,128)(2,1)S(1)}, bf16[4096,256]{1,0:T(8,128)(2,1)}, u32[]{:S(2)}) copy-start(bf16[4096,256]{1,0:T(8,128)(2,1)} %get-tuple-element.91) | copy-start | bytes 6291460

commit v2 on v1

--- a/solution.py
+++ b/solution.py
@@ -21,7 +21,9 @@
 NY, NX, NZ, NC = 4, 4, 8, 2
 NF, NT = NY * NX, NZ * NC
 F32, BF16 = jnp.float32, jnp.bfloat16
-REACH = {(0, 1): 4, (0, -1): 3, (1, 1): 3, (1, -1): 4}
+NH = 4
+PARTS = tuple(range(NH))
+REACH = {(h, way): 4 if (h % 2 == 0) == (way == 1) else 3 for h in PARTS for way in (1, -1)}
 AXES = {"y": "fs_0", "x": "fs_1", "z": "tp_0", "c": "tp_1"}
 
 
@@ -83,29 +85,33 @@
             self.start(h, "p2", a, way)
 
     def step(self, n):
-        for h in (0, 1):
-            if n == 0:
-                for way in (1, -1):
-                    self.start(h, "p1", 0, way)
+        ways, halves = (1, -1), (0, 1)
+        every = [(h, way) for h in halves for way in ways]
+        if n == 0:
+            for h, way in every:
+                self.start(h, "p1", 0, way)
+            for h in halves:
                 self.both(h, 0)
-            elif n == 1:
-                for way in (1, -1):
-                    self.wait(h, "p1", 0, way)
-                    self.start(h, "f1", 0, way)
-                    self.both(h, -way)
-            elif n == 3:
-                for way in (1, -1):
+        elif n == 1:
+            for h, way in every:
+                self.wait(h, "p1", 0, way)
+                self.start(h, "f1", 0, way)
+            for h, way in every:
+                self.both(h, -way)
+        elif n == 3:
+            for h in halves:
+                for way in ways:
                     self.wait(h, "f1", 0, way)
                 self.both(h, 2)
-            elif n == 6:
-                for a in (0, -1, 1, 2):
-                    for way in (1, -1):
-                        self.wait(h, "f2", a, way)
-            else:
-                for a in {2: (0,), 4: (-1, 1), 5: (2,)}[n]:
-                    for way in (1, -1):
-                        self.wait(h, "p2", a, way)
-                        self.start(h, "f2", a, way)
+        elif n == 6:
+            for a in (0, -1, 1, 2):
+                for h, way in every:
+                    self.wait(h, "f2", a, way)
+        else:
+            for a in {2: (0,), 4: (-1, 1), 5: (2,)}[n]:
+                for h, way in every:
+                    self.wait(h, "p2", a, way)
+                    self.start(h, "f2", a, way)
 
     def finish(self):
         for m in self.sent:
@@ -115,10 +121,10 @@
 def exchange_kernel(
     x_hbm, uq_hbm, uk_hbm, h_hbm, ub_hbm, mq_hbm, mk_hbm, mb_hbm, bq_hbm, bk_hbm, bb_hbm,
     qf_hbm, qs_hbm, kf_hbm, ks_hbm, bf_hbm, bs_hbm,
-    qc_out, kc_out, bc_out, lq_out, lk_out, lb_out, clip_out,
-    xv, uv, uqv, ukv, hv, bqv, bkv, bbv, mkv, mbv, qf, qs, kf, ks, bf, bs,
-    g, gb, s1, rr, ss, p2, hi, lo, s2, r2, g3, b3, s4, r4, oq, ok, qd, kd,
-    lsem, dsend, drecv, zs, zr, as_, ar, fwds, fwdr, g1s, g1r, g2s, g2r, ps, pr, osem,
+    oq, ok, bc_out, lq_out, lk_out, lb_out, clip_out,
+    xv, uv, uqv, ukv, hv, bqv, bkv, bbv, mbv, qf, qs, kf, ks, bf, bs,
+    g, gb, s1, rr, ss, p2, hi, lo, s2, r2, g3, b3, s4, r4, qd, kd,
+    lsem, dsend, drecv, zs, zr, as_, ar, fwds, fwdr, g1s, g1r, g2s, g2r, ps, pr,
 ):
     y, x = lax.axis_index("fs_0"), lax.axis_index("fs_1")
     z, c = lax.axis_index("tp_0"), lax.axis_index("tp_1")
@@ -135,7 +141,8 @@
     mine, other = pl.ds(c * 512, 512), pl.ds((1 - c) * 512, 512)
     gq0 = load(mq_hbm.at[:, pl.ds(0, 128)], g.at[f, pl.ds(0, 256)])
     gq1 = load(mq_hbm.at[:, pl.ds(128, 128)], g.at[f, pl.ds(256, 256)])
-    gk = load(mk_hbm, mkv)
+    gk0 = load(mk_hbm.at[:, pl.ds(0, 128)], g.at[f, pl.ds(512, 64)])
+    gk1 = load(mk_hbm.at[:, pl.ds(128, 128)], g.at[f, pl.ds(576, 64)])
     first = [
         load(x_hbm.at[mine], xv.at[c]),
         load(ub_hbm.at[mine], uv.at[c]),
@@ -180,11 +187,10 @@
     ]
     for s in swaps:
         s.start()
-
-    gk.wait()
-    g[f, pl.ds(512, 128)] = jnp.concatenate([mkv[0:128], mkv[128:256]], axis=1)
-    gq0.wait()
-    gq1.wait()
+    ends = [s.wait_send for s in swaps]
+
+    for a in (gq0, gq1, gk0, gk1):
+        a.wait()
     whole = Gather(g, y, x, g1s, g1r)
     whole.step(0)
 
@@ -200,9 +206,9 @@
     )
     for i in range(3):
         for o in range(NZ):
-            for h in (0, 1):
-                at = (2 * o + h) * 32
-                s1[o, h, i * 32 : i * 32 + 32] = proj[i][at : at + 32]
+            for h in PARTS:
+                at = (NH * o + h) * 16
+                s1[o, h, i * 16 : i * 16 + 16] = proj[i][at : at + 16]
 
     def ring(table, h, way, s):
         index = (h * 2 + (0 if way == 1 else 1)) * 4 + s
@@ -212,8 +218,7 @@
         to = {"tp_0": lax.rem(z + (way + NZ), NZ)}
         return remote(src, dst, ring(sends, h, way, s), ring(recvs, h, way, s), to)
 
-    lanes = [(h, way) for h in (0, 1) for way in (1, -1)]
-    zsent = []
+    lanes = [(h, way) for h in PARTS for way in (1, -1)]
     for s in range(4):
         for h, way in lanes:
             reach = REACH[h, way]
@@ -226,43 +231,45 @@
                 zmove(src, ring(rr, h, way, s - 1), zs, zr, h, way, s - 1).wait_recv()
                 src = ring(ss, h, way, s)
                 src[...] = ring(rr, h, way, s - 1)[...] + s1[owner, h]
-            zsent.append((src, ring(rr, h, way, s), zs, zr, h, way, s))
-            zmove(*zsent[-1]).start()
+            move = zmove(src, ring(rr, h, way, s), zs, zr, h, way, s)
+            move.start()
+            ends.append(move.wait_send)
         if s == 2:
             whole.step(1)
     whole.step(2)
-    for h in (0, 1):
+
+    def onward(h, o, index):
+        ref = p2.at[c, o, h]
+        move = remote(ref, ref, fwds.at[h * 8 + index], fwdr.at[h * 8 + index], partner)
+        move.start()
+        ends.append(move.wait_send)
+
+    def along(h, o, way, s):
+        ref = p2.at[c, o, h]
+        move = zmove(ref, ref, as_, ar, h, way, s)
+        move.start()
+        ends.append(move.wait_send)
+
+    for h in PARTS:
         total = s1[z, h]
         for way in (1, -1):
             last = REACH[h, way] - 1
             zmove(s1.at[z, h], ring(rr, h, way, last), zs, zr, h, way, last).wait_recv()
             total = total + ring(rr, h, way, last)[...]
         p2[c, z, h] = total
-
-    def over(h, o, index):
-        ref = p2.at[c, o, h]
-        return remote(ref, ref, fwds.at[h * 8 + index], fwdr.at[h * 8 + index], partner)
-
-    asent, osent = [], []
-
-    def onward(h, o, index):
-        over(h, o, index).start()
-        osent.append((h, o, index))
-
-    for s in range(5):
+        for way in (1, -1):
+            along(h, z, way, 0)
+        onward(h, z, 0)
+    for s in range(1, 5):
         for h, way in lanes:
-            reach = REACH[h, way]
-            if s > reach:
+            if s > REACH[h, way]:
                 continue
             o = lax.rem(z - way * s + NZ, NZ)
             ref = p2.at[c, o, h]
-            if s > 0:
-                zmove(ref, ref, as_, ar, h, way, s - 1).wait_recv()
-            if s < reach:
-                zmove(ref, ref, as_, ar, h, way, s).start()
-                asent.append((ref, ref, as_, ar, h, way, s))
-            if s > 0 or way == 1:
-                onward(h, o, s if way == 1 else NZ - s)
+            zmove(ref, ref, as_, ar, h, way, s - 1).wait_recv()
+            if s < REACH[h, way]:
+                along(h, o, way, s)
+            onward(h, o, s if way == 1 else NZ - s)
         if s == 1:
             whole.step(3)
         if s == 3:
@@ -273,12 +280,12 @@
 
     def spread(half):
         for i in range(3):
-            value = p2[half, :, :, i * 32 : i * 32 + 32].reshape(512, 128)
+            value = p2[half, :, :, i * 16 : i * 16 + 16].reshape(512, 128)
             rows = pl.ds(half * 512, 512)
             hi[i, rows], lo[i, rows] = split(value)
 
     spread(c)
-    for h in (0, 1):
+    for h in PARTS:
         for index in range(NZ):
             o = lax.rem(z - index + NZ, NZ)
             ref = p2.at[1 - c, o, h]
@@ -287,13 +294,13 @@
 
     uq, uk, hh = uqv[...], ukv[...], hv[...]
     low_q = dot(hi[0], uq, 0, 0) + dot(lo[0], uq, 0, 0)
-    low_k = dot(hi[1], uk, 0, 0) + dot(lo[1], uk, 0, 0)
+    low_k = dot(uk, hi[1]) + dot(uk, lo[1])
     low_b = dot(hh, hi[2], 0, 0) + dot(hh, lo[2], 0, 0)
-    low_k = jnp.concatenate([low_k, jnp.zeros((128, 64), F32)], axis=1)
     for p in range(NF):
         s2[p, 0:8] = low_q[8 * p : 8 * p + 8, 0:128]
         s2[p, 8:16] = low_q[8 * p : 8 * p + 8, 128:256]
-        s2[p, 16:24] = low_k[8 * p : 8 * p + 8]
+        s2[p, 16:20] = low_k[4 * p : 4 * p + 4]
+        s2[p, 20:24] = jnp.zeros((4, 128), F32)
         s2[p, 24:40] = low_b[16 * p : 16 * p + 16]
 
     def fs_all(src, dst, k, act):
@@ -323,6 +330,7 @@
     begin = lambda m: m.start()
     left = lambda m: m.wait_send()
     fs_all(lambda p: s2.at[p], r2, 0, begin)
+    ends.append(lambda: fs_all(lambda p: s2.at[p], r2, 0, left))
     r2[f] = s2[f]
     fs_arrive(r2, 0)
     piece = r2[0]
@@ -337,6 +345,8 @@
     g3[f] = piece[0:24]
     tp_all(b3.at[t], b3, 1, begin)
     fs_all(lambda p: g3.at[f], g3, 2, begin)
+    ends.append(lambda: tp_all(b3.at[t], b3, 1, left))
+    ends.append(lambda: fs_all(lambda p: g3.at[f], g3, 2, left))
     tp_arrive(b3, 1)
     tile = b3[0, 16:24]
     for i in range(1, NT):
@@ -345,6 +355,7 @@
         s4[i, 0:16] = b3[i, 0:16]
         s4[i, 16:24] = tile
     fs_all(lambda p: s4.at[p], r4, 3, begin)
+    ends.append(lambda: fs_all(lambda p: s4.at[p], r4, 3, left))
     r4[f] = s4[f]
     fs_arrive(g3, 2)
     whole.step(5)
@@ -373,9 +384,10 @@
     branch.step(0)
 
     low_q = jnp.concatenate([g3[:, 0:8].reshape(128, 128), g3[:, 8:16].reshape(128, 128)], axis=1)
-    low_k = g3[:, 16:24].reshape(128, 128)[:, 0:64]
     lq_out[...] = low_q
-    lk_out[...] = low_k
+    for p in range(NF):
+        lk_out[4 * p : 4 * p + 4] = g3[p, 16:20]
+    low_k = lk_out[...]
     _, _, dir_q = moments(qf[...], qs[...], low_q, clip)
     _, _, dir_k = moments(kf[...], ks[...], low_k, clip)
     qd[0], qd[1] = split(dir_q)
@@ -388,85 +400,65 @@
         step = LEARN * (dot(bq, qd[0]) + dot(bq, qd[1]))
         oq[rows, 0:128] = (g[j, 0:256] - step[:, 0:128]).astype(BF16)
         oq[rows, 128:256] = (g[j, 256:512] - step[:, 128:256]).astype(BF16)
-        step = LEARN * (dot(bk, kd[0]) + dot(bk, kd[1]))
-        pair = g[j, 512:640]
-        ok[rows] = (jnp.concatenate([pair[:, 0:64], pair[:, 64:128]], axis=0) - step).astype(BF16)
-
-    def put(j, act):
-        rows = pl.ds(pl.multiple_of(j * 1024, 1024), 1024)
-        act(pltpu.make_async_copy(oq.at[rows], qc_out.at[rows], osem.at[0, j]))
-        act(pltpu.make_async_copy(ok.at[rows], kc_out.at[rows], osem.at[1, j]))
-
-    for quarter in range(4):
-        pl.loop(quarter * 4, quarter * 4 + 4)(own_columns)
-        put(quarter, begin)
-        branch.step(quarter + 1)
-    branch.step(5)
-    branch.step(6)
-
-    def put_branch(act):
-        @pl.loop(0, 16)
-        def _(j):
-            rows = pl.ds(pl.multiple_of(j * 256, 256), 256)
-            for half in (0, 1):
-                src = gb.at[j, pl.ds(half * 256, 256)]
-                act(pltpu.make_async_copy(src, bc_out.at[rows, pl.ds(half * 128, 128)], osem.at[2 + half, j]))
-
-    put_branch(begin)
-
-    for s in swaps:
-        s.wait_send()
-    for m in zsent + asent:
-        zmove(*m).wait_send()
-    for m in osent:
-        over(*m).wait_send()
-    fs_all(lambda p: s2.at[p], r2, 0, left)
-    tp_all(b3.at[t], b3, 1, left)
-    fs_all(lambda p: g3.at[f], g3, 2, left)
-    fs_all(lambda p: s4.at[p], r4, 3, left)
+        step = LEARN * (dot(kd[0], bk, 1, 1) + dot(kd[1], bk, 1, 1))
+        ok[:, rows] = (jnp.concatenate([g[j, 512:576], g[j, 576:640]], axis=1) - step).astype(BF16)
+
+    done = 0
+    for n, blocks in ((1, 3), (2, 2), (3, 1), (4, 2), (5, 4), (6, 4)):
+        pl.loop(done, done + blocks)(own_columns)
+        done += blocks
+        branch.step(n)
+
+    for m in ends:
+        m()
     whole.finish()
     branch.finish()
-    for quarter in range(4):
-        put(quarter, lambda m: m.wait())
-    put_branch(lambda m: m.wait())
+
+    @pl.loop(0, 16)
+    def _(j):
+        rows = pl.ds(pl.multiple_of(j * 256, 256), 256)
+        bc_out[rows, 0:128] = gb[j, 0:256]
+        bc_out[rows, 128:256] = gb[j, 256:512]
 
 
 def finish_kernel(
-    mq, mk, mb, bq, bk, bb, qf, qs, kf, ks, bf, bs, lq, lk, lb, clip_ref,
+    mq, mk, mb, bq, bk, bb, qf, qs, kf, ks, bf, bs, lq, lk, lb, clip_ref, qc, kc, bc,
     q_step, k_step, b_step, q_new, k_new, b_new, qf_new, qs_new, kf_new, ks_new, bf_new, bs_new,
-    bqv, bkv, bbv, sem,
+    qc_new, kc_new, bc_new, outsem,
 ):
     f = lax.axis_index("fs_0") * NX + lax.axis_index("fs_1")
     t = lax.axis_index("tp_0") * NC + lax.axis_index("tp_1")
-    copies = [
-        pltpu.make_async_copy(src.at[pl.ds(at * 256, 256)], dst, sem.at[i])
-        for i, (src, dst, at) in enumerate(((bq, bqv, f), (bk, bkv, f), (bb, bbv, t)))
+    leaving = [
+        pltpu.make_async_copy(src, dst, outsem.at[i])
+        for i, (src, dst) in enumerate(((qc, qc_new), (kc, kc_new), (bc, bc_new)))
     ]
-    for copy in copies:
-        copy.start()
+    for leave in leaving:
+        leave.start()
     clip = clip_ref[0:1, 0:1]
-    for copy in copies:
-        copy.wait()
+    rows, cols = pl.ds(f * 256, 256), pl.ds(t * 256, 256)
 
     def one(first, second, low, master, basis, first_out, second_out, step_out, new_out, branch):
         first_out[...], second_out[...], way = moments(first[...], second[...], low[...], clip)
         high, rest = split(way)
         if branch:
-            step = dot(high, basis[...], 1, 1) + dot(rest, basis[...], 1, 1)
+            step = dot(high, basis, 1, 1) + dot(rest, basis, 1, 1)
         else:
-            step = dot(basis[...], high) + dot(basis[...], rest)
+            step = dot(basis, high) + dot(basis, rest)
         step_out[...] = step
         new_out[...] = master[...] - LEARN * step
 
-    one(qf, qs, lq, mq, bqv, qf_new, qs_new, q_step, q_new, False)
-    one(kf, ks, lk, mk, bkv, kf_new, ks_new, k_step, k_new, False)
-    one(bf, bs, lb, mb, bbv, bf_new, bs_new, b_step, b_new, True)
+    one(qf, qs, lq, mq, bq[rows], qf_new, qs_new, q_step, q_new, False)
+    one(kf, ks, lk, mk, bk[rows], kf_new, ks_new, k_step, k_new, True)
+    one(bf, bs, lb, mb, bb[cols], bf_new, bs_new, b_step, b_new, True)
+    for leave in leaving:
+        leave.wait()
 
 
 def per_device(*args):
+    args = tuple(a.T if i in (2, 6, 13, 14) else a for i, a in enumerate(args))
     (_, _, _, _, _, mq, mk, mb, bq, bk, bb, qf, qs, kf, ks, bf, bs) = args
     shape = jax.ShapeDtypeStruct
-    hbm = pl.BlockSpec(memory_space=pl.ANY)
+    hbm = pl.BlockSpec(memory_space=pltpu.HBM)
     vmem = pl.BlockSpec(memory_space=pltpu.VMEM)
     v, dma = pltpu.VMEM, pltpu.SemaphoreType.DMA
     qc, kc, bc, lq, lk, lb, clip = pl.pallas_call(
@@ -474,44 +466,46 @@
         name="exchange",
         out_shape=(
             shape((4096, 256), BF16),
-            shape((4096, 64), BF16),
+            shape((64, 4096), BF16),
             shape((4096, 256), BF16),
             shape((128, 256), F32),
-            shape((128, 64), F32),
+            shape((64, 128), F32),
             shape((256, 128), F32),
             shape((8, 128), F32),
         ),
         in_specs=[hbm] * 17,
-        out_specs=(hbm, hbm, hbm, vmem, vmem, vmem, vmem),
+        out_specs=(vmem,) * 7,
         scratch_shapes=[
-            v((2, 512, 256), BF16), v((2, 512, 256), BF16), v((1024, 256), BF16), v((1024, 64), BF16),
+            v((2, 512, 256), BF16), v((2, 512, 256), BF16), v((1024, 256), BF16), v((64, 1024), BF16),
             v((1024, 256), BF16), v((4096, 128), BF16), v((4096, 128), BF16), v((512, 128), BF16),
-            v((256, 64), F32), v((256, 256), F32), v((128, 256), F32), v((128, 256), F32),
-            v((128, 64), F32), v((128, 64), F32), v((256, 128), F32), v((256, 128), F32),
-            v((16, 640, 128), F32), v((16, 512, 128), BF16), v((8, 2, 96, 128), F32),
-            v((16, 96, 128), F32), v((16, 96, 128), F32), v((2, 8, 2, 96, 128), F32),
+            v((256, 256), F32), v((128, 256), F32), v((128, 256), F32),
+            v((64, 128), F32), v((64, 128), F32), v((256, 128), F32), v((256, 128), F32),
+            v((16, 640, 128), F32), v((16, 512, 128), BF16), v((8, NH, 48, 128), F32),
+            v((8 * NH, 48, 128), F32), v((8 * NH, 48, 128), F32), v((2, 8, NH, 48, 128), F32),
             v((3, 1024, 128), BF16), v((3, 1024, 128), BF16), v((16, 40, 128), F32), v((16, 40, 128), F32),
             v((16, 24, 128), F32), v((16, 24, 128), F32), v((16, 24, 128), F32), v((16, 24, 128), F32),
-            v((4096, 256), BF16), v((4096, 64), BF16), v((2, 128, 256), BF16), v((2, 128, 64), BF16),
-            dma((18,)), dma((2,)), dma((2,)), dma((16,)), dma((16,)), dma((16,)), dma((16,)),
-            dma((16,)), dma((16,)), dma((40,)), dma((40,)), dma((40,)), dma((40,)),
-            dma((4, 16)), dma((4, 16)), dma((4, 16)),
+            v((2, 128, 256), BF16), v((2, 64, 128), BF16),
+            dma((19,)), dma((2,)), dma((2,)), dma((8 * NH,)), dma((8 * NH,)), dma((8 * NH,)), dma((8 * NH,)),
+            dma((8 * NH,)), dma((8 * NH,)), dma((40,)), dma((40,)), dma((40,)), dma((40,)),
+            dma((4, 16)), dma((4, 16)),
         ],
         compiler_params=pltpu.CompilerParams(
-            collective_id=0, has_side_effects=True, vmem_limit_bytes=56 * 2**20
+            collective_id=0, has_side_effects=True, vmem_limit_bytes=28 * 2**20
         ),
-    )(*args)
-    qst, kst, bst, qu, ku, bu, qf2, qs2, kf2, ks2, bf2, bs2 = pl.pallas_call(
+    )(*(pltpu.with_memory_space_constraint(a, pltpu.HBM) for a in args))
+    qst, kst, bst, qu, ku, bu, qf2, qs2, kf2, ks2, bf2, bs2, qc, kc, bc = pl.pallas_call(
         finish_kernel,
         name="finish",
         out_shape=tuple(
             shape(a.shape, F32) for a in (mq, mk, mb, mq, mk, mb, qf, qs, kf, ks, bf, bs)
-        ),
-        in_specs=[vmem] * 3 + [hbm] * 3 + [vmem] * 10,
-        out_specs=(vmem,) * 12,
-        scratch_shapes=[v((256, 128), BF16)] * 3 + [dma((3,))],
-    )(mq, mk, mb, bq, bk, bb, qf, qs, kf, ks, bf, bs, lq, lk, lb, clip)
-    return (qst, kst, bst, qu, ku, bu, qc, kc, bc, qf2, qs2, kf2, ks2, bf2, bs2)
+        )
+        + tuple(shape(a.shape, BF16) for a in (qc, kc, bc)),
+        in_specs=[vmem] * 19,
+        out_specs=(vmem,) * 12 + (hbm,) * 3,
+        scratch_shapes=[dma((3,))],
+        compiler_params=pltpu.CompilerParams(vmem_limit_bytes=20 * 2**20),
+    )(mq, mk, mb, bq, bk, bb, qf, qs, kf, ks, bf, bs, lq, lk, lb, clip, qc, kc, bc)
+    return (qst, kst.T, bst, qu, ku.T, bu, qc, kc.T, bc, qf2, qs2, kf2.T, ks2.T, bf2, bs2)
 
 
 def solution(mesh):

time: 110 us -> 86.3 us (0.78)
  local copies, waits for them, and re-layouts: 18.6 us -> 0.05 us
  Pallas kernels: 89.6 us -> 85.4 us
    unnamed x15 -> x24, local copies, waits for them, and re-layouts: 18.6 us -> 0.05 us
    pallas_call x1, Pallas kernels: 85.6 us -> 81.7 us  [per_device(): pl.pallas_call(exchange_kernel, name='exchange', out_shape=(shape((4096,...]
where the time goes in v2:
time: 86.3 us
  Pallas kernels  85.4 us (99%)
    pallas_call x1, Pallas kernels, per_device(): pl.pallas_call(exchange_kernel, name='exchange', out_shape=(shape((4096,...  81.7 us
    pallas_call x1, Pallas kernels, per_device(): pl.pallas_call(finish_kernel, name='finish', out_shape=tuple((shape(a.sha...  3.7 us

profile of v2, /device:TPU:32, one launch (start us, length us, event | category | flops | bytes accessed | tf_op | source)
XLA Modules:
  0.0 86.3 jit_solution(9932766691335136411)
XLA Ops:
  0.7 0.0 copy-start
  0.7 0.0 copy-start.1
  0.7 0.0 copy-start.2
  0.7 0.0 copy-start.3
  0.7 0.0 copy-start.4
  0.7 0.0 copy-start.5
  0.7 0.0 copy-start.6
  0.7 0.0 copy-start.7
  0.7 0.0 copy-start.8
  0.7 0.0 copy-start.9
  0.8 0.0 copy-start.10
  0.8 0.0 copy-start.11
  0.8 81.7 %exchange.1 = (bf16[4096,256]{1,0:T(8,128)(2,1)S(1)}, bf16[64,4096]{1,0:T(8,128)(2,1)S(1)}, bf16[4096,256]{1,0:T(8,128)(2,1)S(1)}, f32[128,256]{1,0:T(8,128)S(1)...) custom-call(bf16[1024,256]{1,0:T(8,128)(2,1)} %x_hbm.1, bf16[1024,256]{1,0:T(8,128)(2,1)} %uq_hbm.1, ...), custom_call_target="tpu_custom_call" | custom-call | tf_op jit(solution)/shard_map/exchange/pallas_call | solution.py:464
  82.4 0.0 copy-done
  82.4 0.0 copy-done.1
  82.5 0.0 copy-done.2
  82.5 0.0 copy-done.3
  82.5 0.0 copy-done.4
  82.5 0.0 copy-done.5
  82.5 0.0 copy-done.6
  82.5 0.0 copy-done.7
  82.5 0.0 copy-done.8
  82.5 0.0 copy-done.9
  82.5 0.0 copy-done.10
  82.5 0.0 copy-done.11
  82.6 3.7 %finish.1 = (f32[256,256]{1,0:T(8,128)}, f32[64,256]{1,0:T(8,128)}, f32[256,256]{1,0:T(8,128)}, f32[256,256]{1,0:T(8,128)}, f32[64,256]{1,0:T(8,128)}, /*index=5...) custom-call(f32[256,256]{1,0:T(8,128)S(1)} %copy-done.3, ...), custom_call_target="tpu_custom_call" | custom-call | tf_op jit(solution)/shard_map/finish/pallas_call | solution.py:496
Async XLA Ops:
  0.7 81.8 %copy-start = (bf16[4096,128]{1,0:T(8,128)(2,1)S(1)}, bf16[4096,128]{1,0:T(8,128)(2,1)}, u32[]{:S(2)}) copy-start(bf16[4096,128]{1,0:T(8,128)(2,1)} %bq.1) | copy-start | bytes 3145732
  0.7 81.8 %copy-start.1 = (bf16[4096,128]{1,0:T(8,128)(2,1)S(1)}, bf16[4096,128]{1,0:T(8,128)(2,1)}, u32[]{:S(2)}) copy-start(bf16[4096,128]{1,0:T(8,128)(2,1)} %bk.1) | copy-start | bytes 3145732
  0.7 81.8 %copy-start.2 = (bf16[4096,128]{1,0:T(8,128)(2,1)S(1)}, bf16[4096,128]{1,0:T(8,128)(2,1)}, u32[]{:S(2)}) copy-start(bf16[4096,128]{1,0:T(8,128)(2,1)} %bb.1) | copy-start | bytes 3145732
  0.7 81.8 %copy-start.3 = (f32[256,256]{1,0:T(8,128)S(1)}, f32[256,256]{1,0:T(8,128)}, u32[]{:S(2)}) copy-start(f32[256,256]{1,0:T(8,128)} %mq.1) | copy-start | bytes 786436
  0.7 81.8 %copy-start.4 = (f32[256,256]{1,0:T(8,128)S(1)}, f32[256,256]{1,0:T(8,128)}, u32[]{:S(2)}) copy-start(f32[256,256]{1,0:T(8,128)} %mb.1) | copy-start | bytes 786436
  0.7 81.8 %copy-start.5 = (f32[128,256]{1,0:T(8,128)S(1)}, f32[128,256]{1,0:T(8,128)}, u32[]{:S(2)}) copy-start(f32[128,256]{1,0:T(8,128)} %qf.1) | copy-start | bytes 393220
  0.7 81.8 %copy-start.6 = (f32[128,256]{1,0:T(8,128)S(1)}, f32[128,256]{1,0:T(8,128)}, u32[]{:S(2)}) copy-start(f32[128,256]{1,0:T(8,128)} %qs.1) | copy-start | bytes 393220
  0.7 81.8 %copy-start.7 = (f32[256,128]{1,0:T(8,128)S(1)}, f32[256,128]{1,0:T(8,128)}, u32[]{:S(2)}) copy-start(f32[256,128]{1,0:T(8,128)} %bf.1) | copy-start | bytes 393220
  0.7 81.8 %copy-start.8 = (f32[256,128]{1,0:T(8,128)S(1)}, f32[256,128]{1,0:T(8,128)}, u32[]{:S(2)}) copy-start(f32[256,128]{1,0:T(8,128)} %bs.1) | copy-start | bytes 393220
  0.7 81.8 %copy-start.9 = (f32[256,64]{0,1:T(8,128)S(1)}, f32[256,64]{0,1:T(8,128)}, u32[]{:S(2)}) copy-start(f32[256,64]{0,1:T(8,128)} %param.23) | copy-start | bytes 196612
  0.8 81.8 %copy-start.10 = (f32[128,64]{0,1:T(8,128)S(1)}, f32[128,64]{0,1:T(8,128)}, u32[]{:S(2)}) copy-start(f32[128,64]{0,1:T(8,128)} %param.30) | copy-start | bytes 98308
  0.8 81.8 %copy-start.11 = (f32[128,64]{0,1:T(8,128)S(1)}, f32[128,64]{0,1:T(8,128)}, u32[]{:S(2)}) copy-start(f32[128,64]{0,1:T(8,128)} %param.31) | copy-start | bytes 98308
